TPU v7x, 32 devices: a whole 2x2x4 slice. The times are simulated.
32 devices in a mesh: ep: 16 (over z, y, x), tp: 2 (over core).
Axes of the slice: x: 2, y: 2, z: 4, core: 2. Of those that a mesh axis runs over, the one named last changes fastest.
Arguments:
- inputs: bfloat16 [256, 1536], P('ep'), may hold values from -6 to 6
- norm_gain_attn: float32 [1536], replicated, may hold values from 0.1 to 1.9
- w_query: bfloat16 [1536, 768], P(None, 'tp'), may hold values from -0.15625 to 0.15625
- w_key: bfloat16 [1536, 128], P(None, 'tp'), may hold values from -0.15625 to 0.15625
- w_value: bfloat16 [1536, 128], P(None, 'tp'), may hold values from -0.15625 to 0.15625
- w_forget: bfloat16 [1536, 12], P(None, 'tp'), may hold values from -0.15625 to 0.15625
- forget_bias: float32 [12], P('tp'), may hold values from 0 to 3
- cache_keys: bfloat16 [256, 2, 1024, 64], P('ep', 'tp'), may hold values from -250 to 250
- cache_values: bfloat16 [256, 2, 1024, 64], P('ep', 'tp'), may hold values from -6 to 6
- cache_gates: float32 [256, 12, 1024], P('ep', 'tp'), as said below
- lengths: int32 [256], P('ep'), may hold values from 128 to 1024, as said below
- w_out: bfloat16 [768, 1536], P('tp'), may hold values from -0.21875 to 0.21875
- norm_gain_ffn: float32 [1536], replicated, may hold values from 0.1 to 1.9
- expert_ids: int32 [256, 6], P('ep'), may hold values from 0 to 15, as said below
- group_weights: float32 [256], P('ep'), may hold values from 0.2 to 1
- expert_weights: float32 [256, 6], P('ep'), may hold values from 0.05 to 1
- exp_gate: bfloat16 [16, 1536, 512], P('ep', None, 'tp'), may hold values from -0.15625 to 0.15625
- exp_up: bfloat16 [16, 1536, 512], P('ep', None, 'tp'), may hold values from -0.15625 to 0.15625
- exp_down: bfloat16 [16, 512, 1536], P('ep', 'tp'), may hold values from -0.25 to 0.25
- dense_gate_vector: float32 [1536], replicated, may hold values from -0.15625 to 0.15625
- dense_gate_w: bfloat16 [1536, 16384], P(None, ('ep', 'tp')), may hold values from -0.15625 to 0.15625
- dense_up_w: bfloat16 [1536, 16384], P(None, ('ep', 'tp')), may hold values from -0.15625 to 0.15625
- dense_down_w: bfloat16 [16384, 1536], P(('ep', 'tp')), may hold values from -0.09375 to 0.09375
Outputs:
- mixed: bfloat16 [256, 1536], P('ep', 'tp')
Inputs may be any that keep to these rules, and one draw needn't show every extreme that they name: `cache_gates`: Non-increasing along positions. `lengths`: some sequence has 1024. `expert_ids`: each row names 6 different experts that share one group (the same quotient by 8). Among the rows of one index of ep at most 12 name the same expert, and some expert is named by exactly 12 rows of every index of ep.
All inputs are finite; a program needn't handle non-finite values.
Results may differ from a plain program's by a relative error of at most 0.013.
Values may be sent and summed in bfloat16 or wider, within the bound.
A program may use at most 128 MiB of HBM per device.

v0:
```python
import functools

import jax
import jax.numpy as jnp
from jax import lax
from jax.experimental import pallas as pl
from jax.experimental.pallas import tpu as pltpu
from jax.sharding import PartitionSpec as P

EPS = 1e-06


def rms_scale(row_block, gain):
    row_block = row_block.astype(jnp.float32)
    factor = lax.rsqrt(jnp.mean(row_block * row_block, axis=-1, keepdims=True) + EPS)
    return (row_block * factor * gain).astype(jnp.bfloat16)


def attend(queries, new_key, new_value, log_forget, keys, values, gates, counts):
    seqs_here, kv_count, group_size, head_size = queries.shape
    cache_positions = lax.broadcasted_iota(jnp.int32, (1, 1, gates.shape[2]), 2)
    last_gate = jnp.sum(
        jnp.where(cache_positions == (counts - 1)[:, None, None], gates, 0.0), axis=2
    )
    offsets = (last_gate + log_forget)[:, :, None] - gates
    offsets = offsets.reshape(seqs_here, kv_count, group_size, gates.shape[2])
    scale_factor = head_size ** (-0.5)
    cached = (
        jnp.einsum("skgd,skld->skgl", queries, keys, preferred_element_type=jnp.float32)
        * scale_factor
        + offsets
    )
    valid_mask = cache_positions.reshape(1, 1, 1, -1) < counts[:, None, None, None]
    cached = jnp.where(valid_mask, cached, -jnp.inf)
    own_score = (
        jnp.einsum("skgd,skd->skg", queries, new_key, preferred_element_type=jnp.float32)
        * scale_factor
    )
    peak_score = jnp.maximum(jnp.max(cached, axis=3), own_score)
    cached_exp = jnp.exp(cached - peak_score[..., None])
    own_exp = jnp.exp(own_score - peak_score)
    denominator = jnp.sum(cached_exp, axis=3) + own_exp
    cached_weight = (cached_exp / denominator[..., None]).astype(jnp.bfloat16)
    own_weight = (own_exp / denominator).astype(jnp.bfloat16)
    mixed_values = jnp.einsum(
        "skgl,skld->skgd", cached_weight, values, preferred_element_type=jnp.float32
    )
    mixed_values = (
        mixed_values
        + own_weight.astype(jnp.float32)[..., None] * new_value.astype(jnp.float32)[:, :, None, :]
    )
    return mixed_values.reshape(seqs_here, kv_count * group_size * head_size).astype(jnp.bfloat16)


MESH = pl.DeviceIdType.MESH


def ffn_kernel(
    n,
    plane,
    heads,
    inp,
    gain,
    dgv,
    ids,
    group_weight,
    expert_weight,
    wo,
    wg,
    wu,
    wd,
    eg,
    eu,
    ed,
    out,
    wo_v,
    wg_v,
    wu_v,
    wd_v,
    eg_v,
    eu_v,
    ed_v,
    xbuf,
    part,
    pbuf,
    aft,
    hid_d,
    hid_e,
    to_pair,
    from_pair,
    own,
    rs_send,
    rs_buf,
    line_send,
    line_buf,
    w_sem,
    pair_sem,
    ag_s,
    ag_r,
    fw_s,
    fw_r,
    rs_s,
    rs_r,
    zag_s,
    zrs_s,
    zrs_r,
):
    me = lax.axis_index("ep")
    depth = n // plane
    z = lax.div(me, plane)
    p = lax.rem(me, plane)
    direction = 1 - 2 * lax.div(2 * z, depth)
    c = lax.axis_index("tp")
    other = 1 - c
    rows, width = inp.shape
    half = width // 2
    total = xbuf.shape[1]
    local_experts = eg.shape[0]
    n_experts = n * local_experts

    loads = [
        pltpu.make_async_copy(hbm, vmem, w_sem.at[i])
        for i, (hbm, vmem) in enumerate(
            ((wo, wo_v), (wg, wg_v), (wu, wu_v), (eg, eg_v), (eu, eu_v), (wd, wd_v), (ed, ed_v))
        )
    ]
    for load in loads:
        load.start()

    barrier = pltpu.get_barrier_semaphore()
    pl.semaphore_signal(barrier, inc=1, device_id={"tp": other}, device_id_type=MESH)

    def line_peer(s):
        return lax.rem(z + direction * s + depth, depth)

    def plane_peer(s):
        return lax.rem(p + s, plane)

    def greet_line(s, carry):
        pl.semaphore_signal(
            barrier, inc=1, device_id={"ep": line_peer(s) * plane + p}, device_id_type=MESH
        )
        return carry

    def greet_plane(s, carry):
        pl.semaphore_signal(
            barrier, inc=1, device_id={"ep": z * plane + plane_peer(s)}, device_id_type=MESH
        )
        return carry

    lax.fori_loop(1, depth, greet_line, 0)
    lax.fori_loop(1, plane, greet_plane, 0)

    side_width = xbuf.shape[2] - half
    lanes = lax.broadcasted_iota(jnp.int32, (rows, side_width), 1)
    row_index = lax.broadcasted_iota(jnp.int32, (rows, rows), 0)
    column_index = lax.broadcasted_iota(jnp.int32, (rows, rows), 1)
    diagonal = row_index == column_index

    def column(row):
        return jnp.sum(jnp.where(diagonal, row, 0.0), axis=1, keepdims=True)

    group = group_weight[...][None, :]
    lane_values = lanes.astype(jnp.float32)
    route = jnp.zeros((rows, side_width), jnp.float32)
    for k in range(ids.shape[0]):
        choice = column(ids[k : k + 1, :].astype(jnp.float32))
        weight = column(group * expert_weight[k : k + 1, :])
        route = jnp.where(lane_values == choice, weight, route)

    loads[0].wait()
    part[...] = jnp.dot(heads[...], wo_v[...], preferred_element_type=jnp.float32).astype(
        jnp.bfloat16
    )
    pl.semaphore_wait(barrier, depth + plane - 1)

    swap = pltpu.make_async_remote_copy(
        src_ref=part,
        dst_ref=pbuf,
        send_sem=pair_sem.at[0],
        recv_sem=pair_sem.at[1],
        device_id={"tp": other},
        device_id_type=MESH,
    )
    swap.start()
    swap.wait_recv()

    after = inp[...].astype(jnp.float32) + (
        part[...].astype(jnp.float32) + pbuf[...].astype(jnp.float32)
    )
    aft[...] = after
    factor = lax.rsqrt(jnp.mean(after * after, axis=-1, keepdims=True) + EPS)
    normed = (after * factor * gain[...][None, :]).astype(jnp.bfloat16)
    logit = jnp.sum(normed.astype(jnp.float32) * dgv[...][None, :], axis=-1, keepdims=True)
    gating = 1.0 / (1.0 + jnp.exp(-logit))
    side = jnp.where(lanes == n_experts, gating, route)
    side_high = side.astype(jnp.bfloat16)
    side_low = (side - side_high.astype(jnp.float32)).astype(jnp.bfloat16)

    def block(j):
        return pl.ds(pl.multiple_of(j * rows, rows), rows)

    xbuf[0, block(me), :half] = normed[:, :half]
    xbuf[1, block(me), :half] = normed[:, half:]
    xbuf[0, block(me), half:] = side_high
    xbuf[1, block(me), half:] = side_low

    def line_copy(source, target):
        index = source * plane + p
        return pltpu.make_async_remote_copy(
            src_ref=xbuf.at[c, block(index)],
            dst_ref=xbuf.at[c, block(index)],
            send_sem=zag_s.at[target],
            recv_sem=ag_r.at[index],
            device_id={"ep": target * plane + p},
            device_id_type=MESH,
        )

    def plane_copy(level, source, target):
        index = level * plane + source
        return pltpu.make_async_remote_copy(
            src_ref=xbuf.at[c, block(index)],
            dst_ref=xbuf.at[c, block(index)],
            send_sem=ag_s.at[level * plane + target],
            recv_sem=ag_r.at[index],
            device_id={"ep": z * plane + target},
            device_id_type=MESH,
        )

    def forward_copy(source, part_index):
        return pltpu.make_async_remote_copy(
            src_ref=xbuf.at[part_index, block(source)],
            dst_ref=xbuf.at[part_index, block(source)],
            send_sem=fw_s.at[source],
            recv_sem=fw_r.at[source],
            device_id={"tp": other},
            device_id_type=MESH,
        )

    def spread_plane(level):
        def body(s, carry):
            plane_copy(level, p, plane_peer(s)).start()
            return carry

        lax.fori_loop(1, plane, body, 0)

    def spread_line(s, carry):
        line_copy(z, line_peer(s)).start()
        return carry

    lax.fori_loop(1, depth, spread_line, 0)
    spread_plane(z)

    def pass_on(s, carry):
        level = line_peer(s)
        line_copy(level, z).wait_recv()
        spread_plane(level)
        forward_copy(level * plane + p, c).start()
        return carry

    lax.fori_loop(1, depth, pass_on, 0)

    def take_plane(t, carry):
        level = line_peer(lax.div(t, plane - 1))
        source = plane_peer(1 + lax.rem(t, plane - 1))
        plane_copy(level, source, p).wait_recv()
        forward_copy(level * plane + source, c).start()
        return carry

    lax.fori_loop(0, depth * (plane - 1), take_plane, 0)

    for load in loads[1:5]:
        load.wait()

    def arrive(s, carry):
        forward_copy(lax.rem(me + n - s, n), other).wait_recv()
        return carry

    lax.fori_loop(1, n, arrive, 0)

    chunk = min(total, 256)

    def pick(values, lane):
        index = lax.broadcasted_iota(jnp.int32, values.shape, 1)
        return jnp.sum(jnp.where(index == lane, values, 0.0), axis=1, keepdims=True)

    def dot(a, b):
        return jnp.dot(a, b, preferred_element_type=jnp.float32)

    def hidden(q, carry):
        at = pl.ds(pl.multiple_of(q * chunk, chunk), chunk)
        x0 = xbuf[0, at, :half]
        x1 = xbuf[1, at, :half]
        sides = xbuf[0, at, half:].astype(jnp.float32) + xbuf[1, at, half:].astype(jnp.float32)
        gate = dot(x0, wg_v[:half]) + dot(x1, wg_v[half:])
        up = dot(x0, wu_v[:half]) + dot(x1, wu_v[half:])
        hid_d[at, :] = (gate / (1.0 + jnp.exp(-gate)) * up * pick(sides, n_experts)).astype(
            jnp.bfloat16
        )
        for e in range(local_experts):
            gate = dot(x0, eg_v[e, :half]) + dot(x1, eg_v[e, half:])
            up = dot(x0, eu_v[e, :half]) + dot(x1, eu_v[e, half:])
            weight = pick(sides, me * local_experts + e)
            hid_e[e, at, :] = (gate / (1.0 + jnp.exp(-gate)) * up * weight).astype(jnp.bfloat16)
        return carry

    def down(at, side_index):
        columns = pl.ds(pl.multiple_of(side_index * half, 128), half)
        result = dot(hid_d[at, :], wd_v[:, columns])
        for e in range(local_experts):
            result += dot(hid_e[e, at, :], ed_v[e, :, columns])
        return result

    def down_pair(q, carry):
        at = pl.ds(pl.multiple_of(q * chunk, chunk), chunk)
        to_pair[at, :] = down(at, other).astype(jnp.bfloat16)
        return carry

    def down_own(q, carry):
        at = pl.ds(pl.multiple_of(q * chunk, chunk), chunk)
        own[at, :] = down(at, c)
        return carry

    def combine(q, carry):
        at = pl.ds(pl.multiple_of(q * chunk, chunk), chunk)
        rs_send[at, :] = (own[at, :] + from_pair[at, :].astype(jnp.float32)).astype(jnp.bfloat16)
        return carry

    chunks = total // chunk
    lax.fori_loop(0, chunks, hidden, 0)
    for load in loads[5:]:
        load.wait()
    lax.fori_loop(0, chunks, down_pair, 0)
    trade = pltpu.make_async_remote_copy(
        src_ref=to_pair,
        dst_ref=from_pair,
        send_sem=pair_sem.at[2],
        recv_sem=pair_sem.at[3],
        device_id={"tp": other},
        device_id_type=MESH,
    )
    trade.start()
    lax.fori_loop(0, chunks, down_own, 0)
    trade.wait_recv()
    lax.fori_loop(0, chunks, combine, 0)

    def share_copy(level, source, target):
        return pltpu.make_async_remote_copy(
            src_ref=rs_send.at[block(level * plane + target)],
            dst_ref=rs_buf.at[block(level * plane + source)],
            send_sem=rs_s.at[level * plane + target],
            recv_sem=rs_r.at[level * plane + source],
            device_id={"ep": z * plane + target},
            device_id_type=MESH,
        )

    def settle_copy(source, target):
        return pltpu.make_async_remote_copy(
            src_ref=line_send.at[block(target)],
            dst_ref=line_buf.at[block(source)],
            send_sem=zrs_s.at[target],
            recv_sem=zrs_r.at[source],
            device_id={"ep": target * plane + p},
            device_id_type=MESH,
        )

    def share(t, carry):
        level = line_peer(depth - 1 - lax.div(t, plane - 1))
        share_copy(level, p, plane_peer(1 + lax.rem(t, plane - 1))).start()
        return carry

    lax.fori_loop(0, depth * (plane - 1), share, 0)

    def plane_sum(level):
        index = level * plane + p
        start = own[block(index), :] + from_pair[block(index), :].astype(jnp.float32)

        def body(s, acc):
            source = plane_peer(s)
            share_copy(level, source, p).wait_recv()
            return acc + rs_buf[block(level * plane + source), :].astype(jnp.float32)

        return lax.fori_loop(1, plane, body, start)

    def settle(s, carry):
        level = line_peer(depth - s)
        line_send[block(level), :] = plane_sum(level).astype(jnp.bfloat16)
        settle_copy(z, level).start()
        return carry

    lax.fori_loop(1, depth, settle, 0)
    columns = pl.ds(pl.multiple_of(c * half, 128), half)
    summed = plane_sum(z) + aft[:, columns]

    def collect(s, acc):
        level = line_peer(s)
        settle_copy(level, z).wait_recv()
        return acc + line_buf[block(level), :].astype(jnp.float32)

    summed = lax.fori_loop(1, depth, collect, summed)
    out[...] = summed.astype(out.dtype)

    swap.wait_send()
    trade.wait_send()

    def finish_line(s, carry):
        peer = line_peer(s)
        line_copy(z, peer).wait_send()
        settle_copy(z, peer).wait_send()
        return carry

    def finish_plane(t, carry):
        level = line_peer(lax.div(t, plane - 1))
        target = plane_peer(1 + lax.rem(t, plane - 1))
        plane_copy(level, p, target).wait_send()
        share_copy(level, p, target).wait_send()
        return carry

    def finish_forward(s, carry):
        forward_copy(lax.rem(me + s, n), c).wait_send()
        return carry

    lax.fori_loop(1, depth, finish_line, 0)
    lax.fori_loop(0, depth * (plane - 1), finish_plane, 0)
    lax.fori_loop(1, n, finish_forward, 0)


def ffn(n, heads, inputs, gain, dgv, ids, group_weight, expert_weight, wo, wg, wu, wd, eg, eu, ed):
    rows, width = inputs.shape
    half = width // 2
    total = n * rows
    plane = 1
    while plane * plane < n:
        plane *= 2
    side_width = (n * eg.shape[0] + 128) // 128 * 128
    dense = wg.shape[1]
    local_experts, _, expert_ff = eg.shape
    bf16, f32 = jnp.bfloat16, jnp.float32
    vmem = pl.BlockSpec(memory_space=pltpu.VMEM)
    hbm = pl.BlockSpec(memory_space=pl.ANY)
    dma = pltpu.SemaphoreType.DMA
    return pl.pallas_call(
        functools.partial(ffn_kernel, n, plane),
        out_shape=jax.ShapeDtypeStruct((rows, half), bf16),
        in_specs=[vmem] * 7 + [hbm] * 7,
        out_specs=vmem,
        scratch_shapes=[
            pltpu.VMEM(wo.shape, bf16),
            pltpu.VMEM(wg.shape, bf16),
            pltpu.VMEM(wu.shape, bf16),
            pltpu.VMEM(wd.shape, bf16),
            pltpu.VMEM(eg.shape, bf16),
            pltpu.VMEM(eu.shape, bf16),
            pltpu.VMEM(ed.shape, bf16),
            pltpu.VMEM((2, total, half + side_width), bf16),
            pltpu.VMEM((rows, width), bf16),
            pltpu.VMEM((rows, width), bf16),
            pltpu.VMEM((rows, width), f32),
            pltpu.VMEM((total, dense), bf16),
            pltpu.VMEM((local_experts, total, expert_ff), bf16),
            pltpu.VMEM((total, half), bf16),
            pltpu.VMEM((total, half), bf16),
            pltpu.VMEM((total, half), f32),
            pltpu.VMEM((total, half), bf16),
            pltpu.VMEM((total, half), bf16),
            pltpu.VMEM((n // plane * rows, half), bf16),
            pltpu.VMEM((n // plane * rows, half), bf16),
            dma((7,)),
            dma((4,)),
            dma((n,)),
            dma((n,)),
            dma((n,)),
            dma((n,)),
            dma((n,)),
            dma((n,)),
            dma((n // plane,)),
            dma((n // plane,)),
            dma((n // plane,)),
        ],
        compiler_params=pltpu.CompilerParams(
            collective_id=0, has_side_effects=True, vmem_limit_bytes=56 * 1024 * 1024
        ),
    )(heads, inputs, gain, dgv, ids, group_weight, expert_weight, wo, wg, wu, wd, eg, eu, ed)


def shards(
    inputs,
    norm_gain_attn,
    w_query,
    w_key,
    w_value,
    w_forget,
    forget_bias,
    cache_keys,
    cache_values,
    cache_gates,
    lengths,
    w_out,
    norm_gain_ffn,
    expert_ids,
    group_weights,
    expert_weights,
    exp_gate,
    exp_up,
    exp_down,
    dense_gate_vector,
    dense_gate_w,
    dense_up_w,
    dense_down_w,
):
    seqs_here, model_width = inputs.shape
    kv_count = cache_keys.shape[1]
    head_size = cache_keys.shape[3]
    heads_here = w_forget.shape[1]
    group_size = heads_here // kv_count
    normed = rms_scale(inputs, norm_gain_attn)
    queries = jnp.dot(normed, w_query, preferred_element_type=jnp.float32).astype(jnp.bfloat16)
    queries = queries.reshape(seqs_here, kv_count, group_size, head_size)
    new_key = (
        jnp.dot(normed, w_key, preferred_element_type=jnp.float32)
        .astype(jnp.bfloat16)
        .reshape(seqs_here, kv_count, head_size)
    )
    new_value = (
        jnp.dot(normed, w_value, preferred_element_type=jnp.float32)
        .astype(jnp.bfloat16)
        .reshape(seqs_here, kv_count, head_size)
    )
    log_forget = jax.nn.log_sigmoid(
        jnp.dot(normed, w_forget, preferred_element_type=jnp.float32) + forget_bias
    )
    heads_out = attend(
        queries, new_key, new_value, log_forget, cache_keys, cache_values, cache_gates, lengths
    )
    return ffn(
        lax.axis_size("ep"),
        heads_out,
        inputs,
        norm_gain_ffn,
        dense_gate_vector,
        expert_ids.T,
        group_weights,
        expert_weights.T,
        w_out,
        dense_gate_w,
        dense_up_w,
        dense_down_w,
        exp_gate,
        exp_up,
        exp_down,
    )


def solution(mesh):
    placed = (
        P("ep", None),
        P(),
        P(None, "tp"),
        P(None, "tp"),
        P(None, "tp"),
        P(None, "tp"),
        P("tp"),
        P("ep", "tp", None, None),
        P("ep", "tp", None, None),
        P("ep", "tp", None),
        P("ep"),
        P("tp", None),
        P(),
        P("ep", None),
        P("ep"),
        P("ep", None),
        P("ep", None, "tp"),
        P("ep", None, "tp"),
        P("ep", "tp", None),
        P(),
        P(None, ("ep", "tp")),
        P(None, ("ep", "tp")),
        P(("ep", "tp"), None),
    )
    return jax.shard_map(
        shards, mesh=mesh, in_specs=placed, out_specs=P("ep", "tp"), check_vma=False
    )
```

profile of v0, /device:TPU:0, one launch (start us, length us, event | category | flops | bytes accessed | tf_op | source)
XLA Modules:
  0.0 41.8 jit_solution(11265930524600326678)
XLA Ops:
  0.0 0.0 copy-start
  0.0 0.0 copy-start.1
  0.0 1.1 %fusion.25 = f32[16]{0:T(128)S(1)} fusion(bf16[16,1536]{1,0:T(8,128)(2,1)} %inp.1), kind=kLoop, calls=%fused_computation.25 | loop fusion | flops 73712 | bytes 49216 | tf_op jit(solution)/shard_map/reduce_sum | solution.py:15
  1.1 1.6 %convolution_convert_fusion = bf16[16,384]{1,0:T(8,128)(2,1)S(1)} fusion(bf16[1536,384]{1,0:T(8,128)(2,1)} %param.25, bf16[16,1536]{1,0:T(8,128)(2,1)} %inp.1, f32[1536]{0:T(1024)} %param.24, f32[16]{0:T(128)S(1)} %add_rsqrt_fusion), kind=kOutput, calls=%fused_computation.9 | convolution fusion | flops 18978816 | bytes 1247296 | tf_op jit(solution)/shard_map/dot_general | solution.py:517
  2.7 0.0 copy-start.2
  2.7 0.0 copy-start.3
  2.7 0.0 copy-start.5
  2.7 0.1 reshape.121
  2.8 0.7 %broadcast_add_fusion = s32[16]{0:T(128)S(1)} fusion(s32[16]{0:T(128)} %param.33), kind=kLoop, calls=%fused_computation.41 | loop fusion | flops 16 | bytes 128 | tf_op jit(solution)/shard_map/sub | solution.py:23
  3.5 0.1 iota_compare_fusion
  3.6 1.1 %select_reduce_fusion = f32[16,6]{0,1:T(8,128)S(1)} fusion(f32[16,6,1024]{2,0,1:T(8,128)} %param.32, pred[16,1024]{1,0:T(8,128)(4,1)S(1)} %iota_compare_fusion), kind=kLoop, calls=%fused_computation.20 | loop fusion | flops 196512 | bytes 409984 | tf_op jit(solution)/shard_map/reduce_sum | solution.py:22
  4.7 1.0 %fusion.32 = f32[16,6]{0,1:T(8,128)S(1)} fusion(f32[16,6]{0,1:T(8,128)S(1)} %select_reduce_fusion, bf16[1536,6]{0,1:T(8,128)(2,1)} %param.28, f32[6]{0:T(128)} %param.29, bf16[16,1536]{1,0:T(8,128)(2,1)} %inp.1, f32[1536]{0:T(1024)} %param.24, f32[16]{0:T(128)S(1)} %add_rsqrt_fusion), kind=kOutput, calls=%fused_computation.38 | convolution fusion | flops 394176 | bytes 74584 | tf_op jit(solution)/shard_map/dot_general | solution.py:530
  5.8 0.0 copy-start.6
  5.8 0.1 copy.26
  5.9 0.8 %iota_compare_fusion.1 = pred[16,1024]{1,0:T(8,128)(4,1)S(1)} fusion(s32[16]{0:T(128)} %param.33), kind=kLoop, calls=%fused_computation.29 | loop fusion | flops 16384 | bytes 16448 | tf_op jit(solution)/shard_map/lt | solution.py:33
  6.6 0.0 copy-done
  6.6 0.0 copy-done.1
  6.6 0.0 copy-start.4
  6.7 0.6 %fusion.38 = (f32[16,6]{1,0:T(8,128)S(1)}, f32[16,6,1024]{2,1,0:T(8,128)S(1)}) fusion(f32[16,6,1024]{2,0,1:T(8,128)S(1)} %copy-done.1, f32[16,6]{1,0:T(8,128)S(1)} %copy.26, bf16[16,6,64]{2,1,0:T(8,128)(2,1)S(1)} %reshape.121, bf16[16,1,1024,64]{2,3,1,0:T(8,128)(2,1)S(1)} %copy-done, pred[16,1024]{1,0:T(8,128)(4,1)S(1)} %iota_compare_fusion.1), kind=kOutput, calls=%fused_computation.42 | convolution fusion | flops 13074336 | bytes 2913024 | tf_op jit(solution)/shard_map/skgd,skld->skgl/dot_general | solution.py:29
  7.3 0.0 copy-done.2
  7.3 0.0 copy-done.3
  7.3 0.0 copy-done.5
  7.3 0.2 fusion.20
  7.5 0.1 fusion.28
  7.6 0.3 fusion.22
  7.9 0.0 copy-done.6
  7.9 0.2 fusion.19
  8.1 0.1 copy-done.4
  8.3 0.7 %fusion.16 = bf16[16,6,64]{2,1,0:T(8,128)(2,1)S(1)} fusion(bf16[16,1,1024,64]{2,3,1,0:T(8,128)(2,1)S(1)} %copy-done.4, f32[16,6,1024]{2,1,0:T(8,128)S(1)} %get-tuple-element.8, f32[16,6]{1,0:T(8,128)S(1)} %get-tuple-element.6, f32[16,6]{1,0:T(8,128)S(1)} %multiply_maximum_fusion, f32[16,64]{1,0:T(8,128)S(1)} %fusion.19, f32[16,6]{1,0:T(8,128)S(1)} %get-tuple-element.5), kind=kOutput, calls=%fused_computation.8 | convolution fusion | flops 12896256 | bytes 2507904 | tf_op jit(solution)/shard_map/skgl,skld->skgd/dot_general | solution.py:45
  9.0 0.7 %convert_element_type.46.heads = bf16[16,384]{1,0:T(8,128)(2,1)} reshape(bf16[16,6,64]{2,1,0:T(8,128)(2,1)S(1)} %fusion.16) | data formatting | bytes 24576 | tf_op jit(solution)/shard_map/convert_element_type | solution.py:52
  9.7 30.8 %shard_map.217 = bf16[16,768]{1,0:T(8,128)(2,1)} custom-call(bf16[16,384]{1,0:T(8,128)(2,1)} %convert_element_type.46.heads, bf16[16,1536]{1,0:T(8,128)(2,1)} %inp.1, f32[1536]{0:T(1024)} %gain.1, f32[1536]{0:T(1024)} %dgv.1, s32[6,16]{1,0:T(8,128)} %bitcast.32, f32[16]{0:T(128)} %group_weight.1, f32[6,16]{1,0:T(8,128)} %bitcast.33, bf16[384,1536]{1,0:T(8,128)(2,1)} %wo.1, ...), custom_call_target="tpu_custom_call" | custom-call | tf_op jit(solution)/shard_map/pallas_call | solution.py:442
  40.4 1.3 %copy.36 = bf16[16,768]{1,0:T(8,128)(2,1)} copy(bf16[16,768]{1,0:T(8,128)(2,1)} %shard_map.217) | data formatting | bytes 49152
  (3 shorter events, 0.0 us)
Async XLA Ops:
  0.0 6.6 %copy-start = (bf16[16,1,1024,64]{2,3,1,0:T(8,128)(2,1)S(1)}, bf16[16,1,1024,64]{2,3,1,0:T(8,128)(2,1)}, u32[]{:S(2)}) copy-start(bf16[16,1,1024,64]{2,3,1,0:T(8,128)(2,1)} %param.30) | copy-start | bytes 6291460
  0.0 6.6 %copy-start.1 = (f32[16,6,1024]{2,0,1:T(8,128)S(1)}, f32[16,6,1024]{2,0,1:T(8,128)}, u32[]{:S(2)}) copy-start(f32[16,6,1024]{2,0,1:T(8,128)} %param.32) | copy-start | bytes 1179652
  2.7 4.5 %copy-start.2 = (bf16[16,1536]{1,0:T(8,128)(2,1)S(1)}, bf16[16,1536]{1,0:T(8,128)(2,1)}, u32[]{:S(2)}) copy-start(bf16[16,1536]{1,0:T(8,128)(2,1)} %inp.1) | copy-start | bytes 147460
  2.7 4.5 %copy-start.3 = (f32[1536]{0:T(1024)S(1)}, f32[1536]{0:T(1024)}, u32[]{:S(2)}) copy-start(f32[1536]{0:T(1024)} %param.24) | copy-start | bytes 18436
  2.7 4.5 %copy-start.5 = (bf16[1536,64]{0,1:T(8,128)(2,1)S(1)}, bf16[1536,64]{0,1:T(8,128)(2,1)}, u32[]{:S(2)}) copy-start(bf16[1536,64]{0,1:T(8,128)(2,1)} %param.26) | copy-start | bytes 589828
  5.8 2.1 %copy-start.6 = (bf16[1536,64]{0,1:T(8,128)(2,1)S(1)}, bf16[1536,64]{0,1:T(8,128)(2,1)}, u32[]{:S(2)}) copy-start(bf16[1536,64]{0,1:T(8,128)(2,1)} %param.27) | copy-start | bytes 589828
  6.6 1.6 %copy-start.4 = (bf16[16,1,1024,64]{2,3,1,0:T(8,128)(2,1)S(1)}, bf16[16,1,1024,64]{2,3,1,0:T(8,128)(2,1)}, u32[]{:S(2)}) copy-start(bf16[16,1,1024,64]{2,3,1,0:T(8,128)(2,1)} %param.31) | copy-start | bytes 6291460
where the time goes:
time: 42.2 us; the launch traced here: 41.8 us
  Pallas kernels  30.8 us (73%)
  matrix products  4.52 us (11%)
  other arithmetic  4 us (9%)
  local copies, waits for them, and re-layouts  2.42 us (6%)
    pallas_call x1, Pallas kernels, ffn(): pl.pallas_call(functools.partial(ffn_kernel, n, plane), out_shape=jax.Sha...  30.8 us
    dot_general x1, matrix products, shards(): jnp.dot(normed, w_query, preferred_element_type=jnp.float32)  1.63 us
    unnamed x15, local copies, waits for them, and re-layouts  1.53 us
    reduce_sum x1, other arithmetic, attend(): jnp.sum(jnp.where(cache_positions == (counts - 1)[:, None, None], gates,...  1.11 us
    reduce_sum x1, other arithmetic, rms_scale(): jnp.mean(row_block * row_block, axis=-1, keepdims=True) + EPS  1.07 us
    dot_general x1, matrix products, shards(): jnp.dot(normed, w_forget, preferred_element_type=jnp.float32) + forget_bias  1.03 us

commit v1 on v0

--- a/solution.py
+++ b/solution.py
@@ -16,55 +16,28 @@
     return (row_block * factor * gain).astype(jnp.bfloat16)
 
 
-def attend(queries, new_key, new_value, log_forget, keys, values, gates, counts):
-    seqs_here, kv_count, group_size, head_size = queries.shape
-    cache_positions = lax.broadcasted_iota(jnp.int32, (1, 1, gates.shape[2]), 2)
-    last_gate = jnp.sum(
-        jnp.where(cache_positions == (counts - 1)[:, None, None], gates, 0.0), axis=2
-    )
-    offsets = (last_gate + log_forget)[:, :, None] - gates
-    offsets = offsets.reshape(seqs_here, kv_count, group_size, gates.shape[2])
-    scale_factor = head_size ** (-0.5)
-    cached = (
-        jnp.einsum("skgd,skld->skgl", queries, keys, preferred_element_type=jnp.float32)
-        * scale_factor
-        + offsets
-    )
-    valid_mask = cache_positions.reshape(1, 1, 1, -1) < counts[:, None, None, None]
-    cached = jnp.where(valid_mask, cached, -jnp.inf)
-    own_score = (
-        jnp.einsum("skgd,skd->skg", queries, new_key, preferred_element_type=jnp.float32)
-        * scale_factor
-    )
-    peak_score = jnp.maximum(jnp.max(cached, axis=3), own_score)
-    cached_exp = jnp.exp(cached - peak_score[..., None])
-    own_exp = jnp.exp(own_score - peak_score)
-    denominator = jnp.sum(cached_exp, axis=3) + own_exp
-    cached_weight = (cached_exp / denominator[..., None]).astype(jnp.bfloat16)
-    own_weight = (own_exp / denominator).astype(jnp.bfloat16)
-    mixed_values = jnp.einsum(
-        "skgl,skld->skgd", cached_weight, values, preferred_element_type=jnp.float32
-    )
-    mixed_values = (
-        mixed_values
-        + own_weight.astype(jnp.float32)[..., None] * new_value.astype(jnp.float32)[:, :, None, :]
-    )
-    return mixed_values.reshape(seqs_here, kv_count * group_size * head_size).astype(jnp.bfloat16)
-
-
 MESH = pl.DeviceIdType.MESH
 
 
-def ffn_kernel(
+def layer_kernel(
     n,
     plane,
-    heads,
-    inp,
-    gain,
-    dgv,
-    ids,
-    group_weight,
-    expert_weight,
+    inp_h,
+    gain_a_h,
+    wq_h,
+    wk_h,
+    wv_h,
+    wf_h,
+    bias_h,
+    keys_h,
+    vals_h,
+    gates_h,
+    lens_h,
+    gain_h,
+    dgv_h,
+    ids_h,
+    group_weight_h,
+    expert_weight_h,
     wo,
     wg,
     wu,
@@ -73,6 +46,25 @@
     eu,
     ed,
     out,
+    inp,
+    gain_a,
+    wq_v,
+    wkv_v,
+    wf_v,
+    bias,
+    keys_v,
+    vals_v,
+    gates_v,
+    lens,
+    gain,
+    dgv,
+    ids,
+    group_weight,
+    expert_weight,
+    spread_q,
+    score,
+    weight_v,
+    mixed_v,
     wo_v,
     wg_v,
     wu_v,
@@ -93,6 +85,7 @@
     rs_buf,
     line_send,
     line_buf,
+    in_sem,
     w_sem,
     pair_sem,
     ag_s,
@@ -124,6 +117,30 @@
             ((wo, wo_v), (wg, wg_v), (wu, wu_v), (eg, eg_v), (eu, eu_v), (wd, wd_v), (ed, ed_v))
         )
     ]
+    head_size = wk_h.shape[0]
+    small = (
+        (inp_h, inp),
+        (gain_a_h, gain_a),
+        (wq_h, wq_v),
+        (wk_h, wkv_v.at[:head_size]),
+        (wv_h, wkv_v.at[head_size:]),
+        (wf_h, wf_v),
+        (bias_h, bias),
+        (lens_h, lens),
+        (gates_h, gates_v),
+        (keys_h, keys_v),
+        (vals_h, vals_v),
+        (gain_h, gain),
+        (dgv_h, dgv),
+        (ids_h, ids),
+        (group_weight_h, group_weight),
+        (expert_weight_h, expert_weight),
+    )
+    brings = [
+        pltpu.make_async_copy(hbm, vmem, in_sem.at[i]) for i, (hbm, vmem) in enumerate(small)
+    ]
+    for bring in brings:
+        bring.start()
     for load in loads:
         load.start()
 
@@ -159,6 +176,77 @@
 
     def column(row):
         return jnp.sum(jnp.where(diagonal, row, 0.0), axis=1, keepdims=True)
+
+    for bring in brings[:8]:
+        bring.wait()
+    normed = rms_scale(inp[...], gain_a[...][None, :])
+    nt = (((1,), (1,)), ((), ()))
+    queries = jnp.dot(normed, wq_v[...], preferred_element_type=jnp.float32)
+    new_kv = lax.dot_general(normed, wkv_v[...], nt, preferred_element_type=jnp.float32)
+    forget = lax.dot_general(normed, wf_v[...], nt, preferred_element_type=jnp.float32)
+    forget = forget + bias[...][None, :]
+    forget = jnp.minimum(forget, 0.0) - jnp.log1p(jnp.exp(-jnp.abs(forget)))
+    queries = queries.astype(jnp.bfloat16).astype(jnp.float32)
+    new_kv = new_kv.astype(jnp.bfloat16).astype(jnp.float32)
+    kv_swapped = pltpu.roll(new_kv, head_size, 1)
+    pair_lane = lax.broadcasted_iota(jnp.int32, new_kv.shape, 1)
+    first = pair_lane < head_size
+    new_key = jnp.where(first, new_kv, kv_swapped)
+    new_value = jnp.where(first, kv_swapped, new_kv)
+    span = rows * head_size
+    own_block = lax.div(
+        lax.broadcasted_iota(jnp.int32, (rows, span), 1), head_size
+    ) == lax.broadcasted_iota(jnp.int32, (rows, span), 0)
+    head_count = wf_h.shape[0]
+    lanes_pair = 2 * head_size
+    own_scores = []
+    scale_factor = head_size ** (-0.5)
+    for h in range(head_count):
+        pair = queries[:, (h // 2) * lanes_pair : (h // 2 + 1) * lanes_pair]
+        swapped = pltpu.roll(pair, head_size, 1)
+        doubled = jnp.where(first, pair, swapped) if h % 2 == 0 else jnp.where(first, swapped, pair)
+        own_scores.append(
+            jnp.sum(jnp.where(first, doubled * new_key, 0.0), axis=1, keepdims=True) * scale_factor
+        )
+        wide = jnp.concatenate([doubled] * (span // lanes_pair), axis=1)
+        spread_q[h * rows : (h + 1) * rows, :] = jnp.where(own_block, wide, 0.0).astype(
+            jnp.bfloat16
+        )
+    for bring in brings[8:10]:
+        bring.wait()
+    score[...] = jnp.dot(spread_q[...], keys_v[...], preferred_element_type=jnp.float32)
+    counts = column(lens[...][None, :].astype(jnp.float32)).astype(jnp.int32)
+    positions = lax.broadcasted_iota(jnp.int32, (rows, gates_v.shape[2]), 1)
+    own_weights = []
+    for h in range(head_count):
+        gates = gates_v[h]
+        last = jnp.sum(jnp.where(positions == counts - 1, gates, 0.0), axis=1, keepdims=True)
+        offsets = (last + forget[:, h : h + 1]) - gates
+        cached = score[h * rows : (h + 1) * rows, :] * scale_factor + offsets
+        cached = jnp.where(positions < counts, cached, -jnp.inf)
+        peak = jnp.maximum(jnp.max(cached, axis=1, keepdims=True), own_scores[h])
+        cached = jnp.exp(cached - peak)
+        own_exp = jnp.exp(own_scores[h] - peak)
+        inverse = 1.0 / (jnp.sum(cached, axis=1, keepdims=True) + own_exp)
+        weight_v[h * rows : (h + 1) * rows, :] = (cached * inverse).astype(jnp.bfloat16)
+        own_weights.append((own_exp * inverse).astype(jnp.bfloat16).astype(jnp.float32))
+    brings[10].wait()
+    mixed_v[...] = lax.dot_general(
+        weight_v[...], vals_v[...], nt, preferred_element_type=jnp.float32
+    )
+    folded = []
+    for h in range(head_count):
+        block_values = jnp.where(own_block, mixed_v[h * rows : (h + 1) * rows, :], 0.0)
+        total_pair = block_values[:, :lanes_pair]
+        for k in range(1, span // lanes_pair):
+            total_pair += block_values[:, k * lanes_pair : (k + 1) * lanes_pair]
+        total_pair += pltpu.roll(total_pair, head_size, 1)
+        folded.append(total_pair + own_weights[h] * new_value)
+    heads = jnp.concatenate(
+        [jnp.where(first, folded[h], folded[h + 1]) for h in range(0, head_count, 2)], axis=1
+    ).astype(jnp.bfloat16)
+    for bring in brings[11:]:
+        bring.wait()
 
     group = group_weight[...][None, :]
     lane_values = lanes.astype(jnp.float32)
@@ -169,7 +257,7 @@
         route = jnp.where(lane_values == choice, weight, route)
 
     loads[0].wait()
-    part[...] = jnp.dot(heads[...], wo_v[...], preferred_element_type=jnp.float32).astype(
+    part[...] = jnp.dot(heads, wo_v[...], preferred_element_type=jnp.float32).astype(
         jnp.bfloat16
     )
     pl.semaphore_wait(barrier, depth + plane - 1)
@@ -425,7 +513,9 @@
     lax.fori_loop(1, n, finish_forward, 0)
 
 
-def ffn(n, heads, inputs, gain, dgv, ids, group_weight, expert_weight, wo, wg, wu, wd, eg, eu, ed):
+def layer(n, *operands):
+    inputs, _, wq, wk, _, wf, bias, keys, _, gates, lens = operands[:11]
+    _, dgv, ids, group_weight, expert_weight, wo, wg, wu, wd, eg, eu, ed = operands[11:]
     rows, width = inputs.shape
     half = width // 2
     total = n * rows
@@ -435,16 +525,41 @@
     side_width = (n * eg.shape[0] + 128) // 128 * 128
     dense = wg.shape[1]
     local_experts, _, expert_ff = eg.shape
+    head_count, _, cache = gates.shape
+    head_size = wk.shape[0]
     bf16, f32 = jnp.bfloat16, jnp.float32
     vmem = pl.BlockSpec(memory_space=pltpu.VMEM)
     hbm = pl.BlockSpec(memory_space=pl.ANY)
     dma = pltpu.SemaphoreType.DMA
+
+    def like(array):
+        return pltpu.VMEM(array.shape, array.dtype)
+
     return pl.pallas_call(
-        functools.partial(ffn_kernel, n, plane),
+        functools.partial(layer_kernel, n, plane),
         out_shape=jax.ShapeDtypeStruct((rows, half), bf16),
-        in_specs=[vmem] * 7 + [hbm] * 7,
+        in_specs=[hbm] * len(operands),
         out_specs=vmem,
         scratch_shapes=[
+            like(inputs),
+            like(dgv),
+            like(wq),
+            pltpu.VMEM((2 * head_size, width), bf16),
+            like(wf),
+            like(bias),
+            like(keys),
+            like(keys),
+            like(gates),
+            like(lens),
+            like(dgv),
+            like(dgv),
+            like(ids),
+            like(group_weight),
+            like(expert_weight),
+            pltpu.VMEM((head_count * rows, rows * head_size), bf16),
+            pltpu.VMEM((head_count * rows, cache), f32),
+            pltpu.VMEM((head_count * rows, cache), bf16),
+            pltpu.VMEM((head_count * rows, rows * head_size), f32),
             pltpu.VMEM(wo.shape, bf16),
             pltpu.VMEM(wg.shape, bf16),
             pltpu.VMEM(wu.shape, bf16),
@@ -465,6 +580,7 @@
             pltpu.VMEM((total, half), bf16),
             pltpu.VMEM((n // plane * rows, half), bf16),
             pltpu.VMEM((n // plane * rows, half), bf16),
+            dma((16,)),
             dma((7,)),
             dma((4,)),
             dma((n,)),
@@ -480,7 +596,12 @@
         compiler_params=pltpu.CompilerParams(
             collective_id=0, has_side_effects=True, vmem_limit_bytes=56 * 1024 * 1024
         ),
-    )(heads, inputs, gain, dgv, ids, group_weight, expert_weight, wo, wg, wu, wd, eg, eu, ed)
+    )(*operands)
+
+
+def stacked(cache):
+    flipped = jnp.swapaxes(cache, 2, 3)
+    return flipped.reshape(-1, flipped.shape[3])
 
 
 def shards(
@@ -508,34 +629,19 @@
     dense_up_w,
     dense_down_w,
 ):
-    seqs_here, model_width = inputs.shape
-    kv_count = cache_keys.shape[1]
-    head_size = cache_keys.shape[3]
-    heads_here = w_forget.shape[1]
-    group_size = heads_here // kv_count
-    normed = rms_scale(inputs, norm_gain_attn)
-    queries = jnp.dot(normed, w_query, preferred_element_type=jnp.float32).astype(jnp.bfloat16)
-    queries = queries.reshape(seqs_here, kv_count, group_size, head_size)
-    new_key = (
-        jnp.dot(normed, w_key, preferred_element_type=jnp.float32)
-        .astype(jnp.bfloat16)
-        .reshape(seqs_here, kv_count, head_size)
-    )
-    new_value = (
-        jnp.dot(normed, w_value, preferred_element_type=jnp.float32)
-        .astype(jnp.bfloat16)
-        .reshape(seqs_here, kv_count, head_size)
-    )
-    log_forget = jax.nn.log_sigmoid(
-        jnp.dot(normed, w_forget, preferred_element_type=jnp.float32) + forget_bias
-    )
-    heads_out = attend(
-        queries, new_key, new_value, log_forget, cache_keys, cache_values, cache_gates, lengths
-    )
-    return ffn(
+    return layer(
         lax.axis_size("ep"),
-        heads_out,
         inputs,
+        norm_gain_attn,
+        w_query,
+        w_key.T,
+        w_value.T,
+        w_forget.T,
+        forget_bias,
+        stacked(cache_keys),
+        stacked(cache_values),
+        jnp.swapaxes(cache_gates, 0, 1),
+        lengths,
         norm_gain_ffn,
         dense_gate_vector,
         expert_ids.T,

time: 42.2 us -> 34.6 us (0.82)
  matrix products: 4.52 us -> 0 us
  other arithmetic: 4 us -> 0 us
  Pallas kernels: 30.8 us -> 33 us
  local copies, waits for them, and re-layouts: 2.42 us -> 1.35 us
    dot_general x7 -> x0, matrix products: 4.52 us -> none  [the longest x1 1.63 us: shards(): jnp.dot(normed, w_query, preferred_element_type=jnp.float32)]
    reduce_sum x3 -> x0, other arithmetic: 2.43 us -> none  [the longest x1 1.11 us: attend(): jnp.sum(jnp.where(cache_positions == (counts - 1)[:, None, None], gates,...]
    pallas_call x1, Pallas kernels: 30.8 us -> 33 us  [layer(): pl.pallas_call(functools.partial(layer_kernel, n, plane), out_shape=jax.S...]
    lt x1 -> x0, other arithmetic: 0.76 us -> none  [attend(): cache_positions.reshape(1, 1, 1, -1) < counts[:, None, None, None]]
    convert_element_type x1 -> x0, local copies, waits for them, and re-layouts: 0.71 us -> none  [attend(): mixed_values.reshape(seqs_here, kv_count * group_size * head_size)]
    sub x1 -> x0, other arithmetic: 0.69 us -> none  [attend(): counts - 1]
    unnamed x15 -> x1, local copies, waits for them, and re-layouts: 1.53 us -> 1.35 us
where the time goes in v1:
time: 34.6 us; the launch traced here: 34.4 us
  Pallas kernels  33 us (95%)
  local copies, waits for them, and re-layouts  1.35 us (4%)
    pallas_call x1, Pallas kernels, layer(): pl.pallas_call(functools.partial(layer_kernel, n, plane), out_shape=jax.S...  33 us
    unnamed x1, local copies, waits for them, and re-layouts  1.35 us

profile of v1, /device:TPU:0, one launch (start us, length us, event | category | flops | bytes accessed | tf_op | source)
XLA Modules:
  0.0 34.4 jit_solution(6581627161157850982)
XLA Ops:
  0.0 33.0 %shard_map.217 = bf16[16,768]{1,0:T(8,128)(2,1)} custom-call(bf16[16,1536]{1,0:T(8,128)(2,1)} %inp_h.1, f32[1536]{0:T(1024)} %gain_a_h.1, bf16[1536,384]{1,0:T(8,128)(2,1)} %wq_h.1, bf16[64,1536]{1,0:T(8,128)(2,1)} %bitcast.15, bf16[64,1536]{1,0:T(8,128)(2,1)} %bitcast.16, bf16[6,1536]{1,0:T(8,128)(2,1)} %bitcast.17, f32[6]{0:T(128)} %bias_h.1, ...), custom_call_target="tpu_custom_call" | custom-call | tf_op jit(solution)/shard_map/pallas_call | solution.py:538
  33.1 1.3 %copy.25 = bf16[16,768]{1,0:T(8,128)(2,1)} copy(bf16[16,768]{1,0:T(8,128)(2,1)} %shard_map.217) | data formatting | bytes 49152
